TPU v7x, 32 devices: a whole 2x2x4 slice. The times are simulated.
32 devices in a mesh: sp: 8 (over z, y), dp: 4 (over x, core).
Axes of the slice: x: 2, y: 2, z: 4, core: 2. Of those that a mesh axis runs over, the one named last changes fastest.
Arguments:
- queries: bfloat16 [16, 16, 512, 128], P('dp', None, 'sp'), may hold values from -6 to 6
- key_maps: bfloat16 [16, 16, 512, 128], P('dp', None, 'sp'), may hold values from -6 to 6
- value_rows: bfloat16 [16, 16, 512, 128], P('dp', None, 'sp'), may hold values from -6 to 6
- gate_logits: bfloat16 [512, 16, 2048], P('sp', 'dp'), may hold values from -6 to 6
- mix_lambda: float32 [16], replicated, may hold values from 0.3 to 0.8
- head_gain: float32 [128], replicated, may hold values from 0.1 to 1.9
- out_weight: bfloat16 [2048, 2048], P('sp', 'dp'), may hold values from -0.125 to 0.125
Outputs:
- projected: bfloat16 [512, 16, 2048], P('sp', 'dp')
All inputs are finite; a program needn't handle non-finite values.
Results may differ from a plain program's by a relative error of at most 0.0075.
Values may be sent and summed in bfloat16 or wider, within the bound.
A program may use at most 64 MiB of HBM per device.

v0:
```python
import jax
import jax.numpy as jnp
from jax import lax
from jax.sharding import PartitionSpec as P

HEAD_DIM = 64
STRETCH = 64
BLOCK = 512


def shortened(shard):
    return jax.tree.map(lambda a: a.astype(jnp.bfloat16) if a.dtype == jnp.float32 else a, shard)


def attend(operands, head_gain):
    query_item, key_item, value_item, weight_two = operands
    length = query_item.shape[0]
    half_cols = query_item.shape[1] // 2
    value_cols = value_item.shape[1]
    block_len = min(BLOCK, length)
    n_blocks = length // block_len
    score_scale = HEAD_DIM ** (-0.5)
    in_segment = jnp.arange(block_len) // STRETCH
    diag_visible = in_segment[None, :] <= in_segment[:, None]

    def query_block(block_index):
        offset = block_index * block_len
        query_rows = lax.dynamic_slice_in_dim(query_item, offset, block_len, 0)

        def update(carry_state, key_block, value_block, visible):
            updated = []
            for which in range(2):
                running, summed, carried = carry_state[which]
                scores = (
                    jnp.dot(
                        query_rows[:, which * half_cols : (which + 1) * half_cols],
                        key_block[:, which * half_cols : (which + 1) * half_cols].T,
                        preferred_element_type=jnp.float32,
                    )
                    * score_scale
                )
                if visible is not None:
                    scores = jnp.where(visible, scores, -1e30)
                highest = jnp.maximum(running, jnp.max(scores, axis=1, keepdims=True))
                rescale = jnp.exp(running - highest)
                weights = jnp.exp(scores - highest)
                summed = summed * rescale + jnp.sum(weights, axis=1, keepdims=True)
                carried = carried * rescale + jnp.dot(
                    weights.astype(jnp.bfloat16), value_block, preferred_element_type=jnp.float32
                )
                updated.append((highest, summed, carried))
            return tuple(updated)

        def advance(key_index, carry_state):
            key_block = lax.dynamic_slice_in_dim(key_item, key_index * block_len, block_len, 0)
            value_block = lax.dynamic_slice_in_dim(value_item, key_index * block_len, block_len, 0)
            return update(carry_state, key_block, value_block, None)

        initial = tuple(
            (
                (
                    jnp.full((block_len, 1), -1e30, jnp.float32),
                    jnp.zeros((block_len, 1), jnp.float32),
                    jnp.zeros((block_len, value_cols), jnp.float32),
                )
                for which in range(2)
            )
        )
        carry_state = lax.fori_loop(0, block_index, advance, initial)
        carry_state = update(
            carry_state,
            lax.dynamic_slice_in_dim(key_item, offset, block_len, 0),
            lax.dynamic_slice_in_dim(value_item, offset, block_len, 0),
            diag_visible,
        )
        combined = carry_state[0][2] / carry_state[0][1] - weight_two * (
            carry_state[1][2] / carry_state[1][1]
        )
        mean_sq = jnp.mean(combined * combined, axis=1, keepdims=True)
        return (combined * lax.rsqrt(mean_sq + 1e-05) * head_gain).astype(jnp.bfloat16)

    pieces = lax.map(query_block, jnp.arange(n_blocks))
    return pieces.reshape(length, value_cols)


def on_device(queries, key_maps, value_rows, gate_logits, mix_lambda, head_gain, out_weight):
    seq_count, head_count, tok_rows, q_cols = queries.shape
    value_cols = value_rows.shape[3]
    item_count = seq_count * head_count
    model_width = gate_logits.shape[2]
    moved = (
        lax.all_to_all(
            queries.reshape(item_count, tok_rows, q_cols),
            "sp",
            split_axis=0,
            concat_axis=1,
            tiled=True,
        ),
        lax.all_to_all(
            key_maps.reshape(item_count, tok_rows, q_cols),
            "sp",
            split_axis=0,
            concat_axis=1,
            tiled=True,
        ),
        lax.all_to_all(
            value_rows.reshape(item_count, tok_rows, value_cols),
            "sp",
            split_axis=0,
            concat_axis=1,
            tiled=True,
        ),
    )
    query_all, key_all, value_all = moved
    per_dev = query_all.shape[0]
    first_item = lax.axis_index("sp") * per_dev
    head_ids = (first_item + jnp.arange(per_dev)) % head_count
    matches = head_ids[:, None] == jnp.arange(head_count)[None, :]
    lambda_local = jnp.sum(jnp.where(matches, mix_lambda[None, :], 0.0), axis=1)

    def attend_one(operands):
        return attend(operands, head_gain)

    normed = lax.map(attend_one, (query_all, key_all, value_all, lambda_local))
    returned = lax.all_to_all(
        shortened(jnp.swapaxes(normed, 0, 1)), "sp", split_axis=0, concat_axis=1, tiled=True
    )
    by_token = returned.reshape(tok_rows, seq_count, model_width)
    gated = (jax.nn.sigmoid(gate_logits.astype(jnp.float32)) * by_token.astype(jnp.float32)).astype(
        jnp.bfloat16
    )
    gated_rows = gated.reshape(tok_rows * seq_count, model_width)
    gathered = lax.all_gather(out_weight, "sp", axis=0, tiled=True)
    result = jnp.dot(
        gated_rows,
        lax.all_gather(gathered, "dp", axis=1, tiled=True),
        preferred_element_type=jnp.float32,
    )
    return result.astype(jnp.bfloat16).reshape(tok_rows, seq_count, model_width)


def solution(mesh):
    placed = (
        P("dp", None, "sp", None),
        P("dp", None, "sp", None),
        P("dp", None, "sp", None),
        P("sp", "dp", None),
        P(),
        P(),
        P("sp", "dp"),
    )
    return jax.shard_map(
        on_device, mesh=mesh, in_specs=placed, out_specs=P("sp", "dp", None), check_vma=False
    )
```

profile of v0, /device:TPU:0, one launch (start us, length us, event | category | flops | bytes accessed | tf_op | source)
XLA Modules:
  0.0 221.4 jit_solution(4606228928445615071)
XLA Ops:
  6.5 33.1 %all_to_all.63 = bf16[64,64,128]{2,1,0:T(8,128)(2,1)S(1)} all-to-all(bf16[64,64,128]{2,1,0:T(8,128)(2,1)} %bitcast.57), channel_id=1, replica_groups=mesh['sp'=8,'dp'=4] {'sp'}, dimensions={0} | all-to-all | bytes 2097152 | tf_op jit(solution)/shard_map/all_to_all | solution.py:99
  39.6 3.7 %all-to-all-start.2 = ((bf16[64,64,128]{2,1,0:T(8,128)(2,1)}), bf16[64,64,128]{2,1,0:T(8,128)(2,1)S(1)}, u32[]{:S(2)}, u32[]{:S(2)}) async-start(bf16[64,64,128]{2,1,0:T(8,128)(2,1)} %bitcast.13), calls=%async_computation.2 | async-start | bytes 2097152 | tf_op jit(solution)/shard_map/all_to_all | solution.py:106
  43.4 0.7 all-gather.3.cloned.1.call-update
  44.1 33.3 %all-to-all-done.2 = bf16[64,64,128]{2,1,0:T(8,128)(2,1)S(1)} async-done(((bf16[64,64,128]{2,1,0:T(8,128)(2,1)}), bf16[64,64,128]{2,1,0:T(8,128)(2,1)S(1)}, u32[]{:S(2)}, u32[]{:S(2)}) %all-to-all-start.2) | async-done | bytes 1048608 | tf_op jit(solution)/shard_map/all_to_all | solution.py:106
  77.3 3.6 %all-to-all-start = ((bf16[64,64,128]{2,1,0:T(8,128)(2,1)}), bf16[64,64,128]{2,1,0:T(8,128)(2,1)S(1)}, u32[]{:S(2)}, u32[]{:S(2)}) async-start(bf16[64,64,128]{2,1,0:T(8,128)(2,1)} %bitcast.58), calls=%async_computation | async-start | bytes 2097152 | tf_op jit(solution)/shard_map/all_to_all | solution.py:92
  81.2 1.1 copy.16
  82.2 1.1 copy.17
  83.3 40.0 %all-to-all-done = bf16[64,64,128]{2,1,0:T(8,128)(2,1)S(1)} async-done(((bf16[64,64,128]{2,1,0:T(8,128)(2,1)}), bf16[64,64,128]{2,1,0:T(8,128)(2,1)S(1)}, u32[]{:S(2)}, u32[]{:S(2)}) %all-to-all-start) | async-done | bytes 1048608 | tf_op jit(solution)/shard_map/all_to_all | solution.py:92
  123.4 1.1 copy-done
  124.5 47.8 %while.86 = (s32[]{:T(128)}, bf16[8,512,128]{1,2,0:T(8,128)(2,1)S(1)}, bf16[8,512,128]{2,1,0:T(8,128)(2,1)S(1)}, bf16[8,512,128]{2,1,0:T(8,128)(2,1)}, bf16[8,51...) while((s32[]{:T(128)}, bf16[8,512,128]{1,2,0:T(8,128)(2,1)S(1)}, ...), condition=%wide.region_7.8_spmd, body=%wide.region_1.7_spmd.sunk | while | flops 206249472 | bytes 8851561 | solution.py:124
  124.5 0.9 dynamic-slice_bitcast_fusion.3
  125.5 0.4 fusion.50
  126.1 0.3 fusion.47
  126.6 1.2 fusion.49
  127.9 0.6 dynamic_slice.56
  128.4 1.9 multiply_reduce_fusion.2
  130.5 1.0 dynamic-slice_bitcast_fusion.3
  131.5 0.4 fusion.50
  132.1 0.3 fusion.47
  132.6 1.3 fusion.49
  133.9 0.6 dynamic_slice.56
  134.5 1.9 multiply_reduce_fusion.2
  136.6 0.9 dynamic-slice_bitcast_fusion.3
  137.5 0.4 fusion.50
  138.1 0.3 fusion.47
  138.7 1.2 fusion.49
  139.9 0.6 dynamic_slice.56
  140.5 1.9 multiply_reduce_fusion.2
  142.5 0.9 dynamic-slice_bitcast_fusion.3
  143.5 0.4 fusion.50
  144.1 0.3 fusion.47
  144.6 1.2 fusion.49
  145.9 0.6 dynamic_slice.56
  146.5 1.9 multiply_reduce_fusion.2
  148.5 0.9 dynamic-slice_bitcast_fusion.3
  149.4 0.4 fusion.50
  150.0 0.3 fusion.47
  150.6 1.2 fusion.49
  151.8 0.6 dynamic_slice.56
  152.4 1.9 multiply_reduce_fusion.2
  154.4 0.9 dynamic-slice_bitcast_fusion.3
  155.4 0.4 fusion.50
  156.0 0.3 fusion.47
  156.5 1.2 fusion.49
  157.8 0.6 dynamic_slice.56
  158.4 1.9 multiply_reduce_fusion.2
  160.4 0.9 dynamic-slice_bitcast_fusion.3
  161.3 0.4 fusion.50
  162.0 0.3 fusion.47
  162.5 1.2 fusion.49
  163.7 0.6 dynamic_slice.56
  164.3 1.9 multiply_reduce_fusion.2
  166.4 0.9 dynamic-slice_bitcast_fusion.3
  167.3 0.4 fusion.50
  167.9 0.3 fusion.47
  168.5 1.2 fusion.49
  169.7 0.6 dynamic_slice.56
  170.3 1.9 multiply_reduce_fusion.2
  172.3 0.8 copy.18
  173.1 29.4 %all_to_all.64 = bf16[512,8,128]{2,1,0:T(8,128)(2,1)S(1)} all-to-all(bf16[512,8,128]{2,1,0:T(8,128)(2,1)S(1)} %bitcast.54), channel_id=1, replica_groups=mesh['sp'=8,'dp'=4] {'sp'}, dimensions={0} | all-to-all | bytes 2097152 | tf_op jit(solution)/shard_map/all_to_all | solution.py:125
  202.9 1.7 reshape.107
  204.6 2.7 %fusion.31 = bf16[64,4,2048]{2,1,0:T(4,128)(2,1)S(1)} fusion(f32[64,4,2048]{2,1,0:T(4,128)} %reshape.107, bf16[64,4,2048]{2,1,0:T(4,128)(2,1)S(1)} %copy-done.1), kind=kLoop, calls=%fused_computation.51 | loop fusion | flops 3145728 | bytes 4194304 | tf_op jit(solution)/shard_map/convert_element_type | solution.py:129
  207.6 5.7 %convolution_convert_fusion = bf16[256,2048]{1,0:T(8,128)(2,1)S(1)} fusion(bf16[256,2048]{1,0:T(8,128)(2,1)S(1)} %reshape.103, bf16[2048,2048]{1,0:T(8,128)(2,1)} %all-gather.5.cloned.1.call-done), kind=kOutput, calls=%fused_computation.48 | convolution fusion | flops 2148007936 | bytes 10485760 | tf_op jit(solution)/shard_map/dot_general | solution.py:134
  213.4 1.2 reshape.104
  (91 shorter events, 5.3 us)
Async XLA Ops:
  39.6 41.4 %copy-start.3 = (f32[16]{0:T(128)S(1)}, f32[16]{0:T(128)}, u32[]{:S(2)}) copy-start(f32[16]{0:T(128)} %param.13) | copy-start | bytes 196
  39.6 37.7 %all-to-all-start.2 = ((bf16[64,64,128]{2,1,0:T(8,128)(2,1)}), bf16[64,64,128]{2,1,0:T(8,128)(2,1)S(1)}, u32[]{:S(2)}, u32[]{:S(2)}) async-start(bf16[64,64,128]{2,1,0:T(8,128)(2,1)} %bitcast.13), calls=%async_computation.2 | async-start | bytes 2097152 | tf_op jit(solution)/shard_map/all_to_all | solution.py:106
  43.3 80.1 %all-gather.3.cloned.1.call-start = ((), (), s32[]{:S(2)}) async-start(), calls=%async_computation.4 | async-start | bytes 2359296 | tf_op jit(solution)/shard_map/all_gather | solution.py:133
  77.3 46.0 %all-to-all-start = ((bf16[64,64,128]{2,1,0:T(8,128)(2,1)}), bf16[64,64,128]{2,1,0:T(8,128)(2,1)S(1)}, u32[]{:S(2)}, u32[]{:S(2)}) async-start(bf16[64,64,128]{2,1,0:T(8,128)(2,1)} %bitcast.58), calls=%async_computation | async-start | bytes 2097152 | tf_op jit(solution)/shard_map/all_to_all | solution.py:92
  80.9 126.7 %all-gather.5.cloned.1.call-start = ((), (), s32[]{:S(2)}) async-start(), calls=%async_computation.5 | async-start | bytes 10485760 | tf_op jit(solution)/shard_map/all_gather | solution.py:136
  123.3 1.2 copy-start
  123.3 1.2 copy-start.2
  202.9 1.7 copy-start.1
Sparse Core Ops, SparseCore 0:
  46.3 75.0 all-gather.2
  123.6 57.2 all-gather.4
where the time goes:
time: 222 us; the launch traced here: 221 us
  waiting for transfers between devices  74 us (33%)
  blocking collectives  62.5 us (28%)
  matrix products  36.6 us (16%)
  local copies, waits for them, and re-layouts  19.7 us (9%)
  between operations  13.5 us (6%)
  starting transfers between devices  7.36 us (3%)
  other arithmetic  7.2 us (3%)
    all_to_all x1, waiting for transfers between devices, on_device(): lax.all_to_all(queries.reshape(item_count, tok_rows, q_cols), 'sp', split...  40 us
    all_to_all x1, waiting for transfers between devices, on_device(): lax.all_to_all(value_rows.reshape(item_count, tok_rows, value_cols), 'sp'...  33.3 us
    all_to_all x1, blocking collectives, on_device(): lax.all_to_all(key_maps.reshape(item_count, tok_rows, q_cols), 'sp', spli...  33.1 us
    all_to_all x1, blocking collectives, on_device(): lax.all_to_all(shortened(jnp.swapaxes(normed, 0, 1)), 'sp', split_axis=0,...  29.4 us
    dot_general x16, matrix products, update(): jnp.dot(weights.astype(jnp.bfloat16), value_block, preferred_element_type...  25.1 us
    squeeze x8, local copies, waits for them, and re-layouts, on_device(): normed = lax.map(attend_one, (query_all, key_all, value_all, lambda_local))  7.44 us
    dot_general x16, matrix products, update(): jnp.dot(query_rows[:, which * half_cols:(which + 1) * half_cols], key_blo...  5.72 us
    dot_general x1, matrix products, on_device(): jnp.dot(gated_rows, lax.all_gather(gathered, 'dp', axis=1, tiled=True), p...  5.71 us
  transfers between devices with their start and end apart: 4, of which 2 were waited for; matrix products, arithmetic and copies ran while one was open for 25% of the time, Pallas kernels for 0%

commit v1 on v0

v1 whole, which is shorter than its diff:
```python
import functools

import jax
import jax.numpy as jnp
from jax import lax
from jax.experimental import pallas as pl
from jax.experimental.pallas import tpu as pltpu
from jax.sharding import PartitionSpec as P

HEAD_DIM = 64
STRETCH = 64
LOG2E = 1.4426950408889634


def attend_item(q, k, v, weight_two, gain, store):
    length, cols = q.shape
    block = min(2 * STRETCH, length)
    factor = HEAD_DIM ** (-0.5) * LOG2E
    first_map = lax.broadcasted_iota(jnp.int32, (block, cols), 1) < cols // 2
    row_seg = (lax.broadcasted_iota(jnp.int32, (2 * block, block), 0) % block) // STRETCH
    col_seg = lax.broadcasted_iota(jnp.int32, (2 * block, block), 1) // STRETCH
    visible = col_seg <= row_seg
    for lo in range(0, length, block):
        hi = lo + block
        rows = q[lo:hi]
        zero = jnp.zeros_like(rows)
        both = jnp.concatenate([jnp.where(first_map, rows, zero), jnp.where(first_map, zero, rows)], axis=0)
        scores = lax.dot_general(
            both, k[:hi], (((1,), (1,)), ((), ())), preferred_element_type=jnp.float32
        )
        diag = jnp.where(visible, scores[:, lo:], -1e30)
        scores = jnp.concatenate([scores[:, :lo], diag], axis=1) if lo else diag
        highest = jnp.max(scores, axis=1, keepdims=True)
        weights = jnp.exp2((scores - highest) * factor)
        summed = jnp.sum(weights, axis=1, keepdims=True)
        mapped = (
            jnp.dot(weights.astype(jnp.bfloat16), v[:hi], preferred_element_type=jnp.float32) / summed
        )
        combined = mapped[:block] - weight_two * mapped[block:]
        mean_sq = jnp.mean(combined * combined, axis=1, keepdims=True)
        store(lo, (combined * lax.rsqrt(mean_sq + 1e-05) * gain).astype(jnp.bfloat16))


def exchange_kernel(n, heads, q_ref, k_ref, v_ref, lam_ref, gain_ref, ret_ref, recv, staged, send_sem, recv_sem, back_sem, ret_sem):
    me = lax.axis_index("sp")
    items, toks, cols = q_ref.shape
    per_dev = items // n
    length = n * toks

    barrier = pltpu.get_barrier_semaphore()

    def greet(step, carry):
        pl.semaphore_signal(barrier, inc=1, device_id={"sp": lax.rem(me + step, n)})
        return carry

    lax.fori_loop(1, n, greet, 0)
    pl.semaphore_wait(barrier, n - 1)

    def send_item(j, carry):
        for which, ref in enumerate((q_ref, k_ref, v_ref)):
            pltpu.make_async_copy(
                ref.at[me * per_dev + j], recv.at[j, which, me], recv_sem.at[j]
            ).start()

        def to_peer(step, carry):
            peer = lax.rem(me + step, n)
            for which, ref in enumerate((q_ref, k_ref, v_ref)):
                pltpu.make_async_remote_copy(
                    src_ref=ref.at[peer * per_dev + j],
                    dst_ref=recv.at[j, which, me],
                    send_sem=send_sem.at[j],
                    recv_sem=recv_sem.at[j],
                    device_id={"sp": peer},
                ).start()
            return carry

        return lax.fori_loop(1, n, to_peer, carry)

    lax.fori_loop(0, per_dev, send_item, 0)

    gain = gain_ref[...]

    def work_item(j, carry):
        pltpu.make_async_copy(recv.at[j], recv.at[j], recv_sem.at[j]).wait()
        q = recv[j, 0].reshape(length, cols)
        k = recv[j, 1].reshape(length, cols)
        v = recv[j, 2].reshape(length, cols)
        item = me * per_dev + j

        def store(lo, rows):
            for r in range(0, rows.shape[0], toks):
                staged[j, (lo + r) // toks] = rows[r : r + toks]

        attend_item(q, k, v, lam_ref[lax.rem(item, heads)], gain, store)
        pltpu.make_async_copy(staged.at[j, me], ret_ref.at[item], ret_sem).start()

        def to_peer(step, carry):
            peer = lax.rem(me + step, n)
            pltpu.make_async_remote_copy(
                src_ref=staged.at[j, peer],
                dst_ref=ret_ref.at[item],
                send_sem=back_sem,
                recv_sem=ret_sem,
                device_id={"sp": peer},
            ).start()
            return carry

        return lax.fori_loop(1, n, to_peer, carry)

    lax.fori_loop(0, per_dev, work_item, 0)
    pltpu.make_async_copy(ret_ref, ret_ref, ret_sem).wait()
    others = staged.at[:, pl.ds(0, n - 1)]
    pltpu.make_async_copy(others, others, back_sem).wait()

    def drain(j, carry):
        for which in range(3):
            part = recv.at[j, which, pl.ds(0, n - 1)]
            pltpu.make_async_copy(part, part, send_sem.at[j]).wait()
        return carry

    lax.fori_loop(0, per_dev, drain, 0)


def on_device(n, queries, key_maps, value_rows, gate_logits, mix_lambda, head_gain, out_weight):
    seqs, heads, toks, cols = queries.shape
    items = seqs * heads
    per_dev = items // n
    width = gate_logits.shape[2]
    anywhere = pl.BlockSpec(memory_space=pl.ANY)
    in_vmem = pl.BlockSpec(memory_space=pltpu.VMEM)
    returned = pl.pallas_call(
        functools.partial(exchange_kernel, n, heads),
        out_shape=jax.ShapeDtypeStruct((items, toks, cols), jnp.bfloat16),
        in_specs=[anywhere, anywhere, anywhere, pl.BlockSpec(memory_space=pltpu.SMEM), in_vmem],
        out_specs=in_vmem,
        scratch_shapes=[
            pltpu.VMEM((per_dev, 3, n, toks, cols), jnp.bfloat16),
            pltpu.VMEM((per_dev, n, toks, cols), jnp.bfloat16),
            pltpu.SemaphoreType.DMA((per_dev,)),
            pltpu.SemaphoreType.DMA((per_dev,)),
            pltpu.SemaphoreType.DMA,
            pltpu.SemaphoreType.DMA,
        ],
        compiler_params=pltpu.CompilerParams(
            collective_id=0, has_side_effects=True, vmem_limit_bytes=40 * 2**20
        ),
        cost_estimate=pl.CostEstimate(flops=5 * 10**10, bytes_accessed=2**28, transcendentals=0),
    )(
        queries.reshape(items, toks, cols),
        key_maps.reshape(items, toks, cols),
        value_rows.reshape(items, toks, cols),
        mix_lambda,
        head_gain.reshape(1, cols),
    )
    by_token = jnp.transpose(returned.reshape(seqs, heads, toks, cols), (2, 0, 1, 3)).reshape(
        toks, seqs, width
    )
    gated = (jax.nn.sigmoid(gate_logits.astype(jnp.float32)) * by_token.astype(jnp.float32)).astype(
        jnp.bfloat16
    )
    gathered = lax.all_gather(out_weight, "sp", axis=0, tiled=True)
    result = jnp.dot(
        gated.reshape(toks * seqs, width),
        lax.all_gather(gathered, "dp", axis=1, tiled=True),
        preferred_element_type=jnp.float32,
    )
    return result.astype(jnp.bfloat16).reshape(toks, seqs, width)


def solution(mesh):
    placed = (
        P("dp", None, "sp", None),
        P("dp", None, "sp", None),
        P("dp", None, "sp", None),
        P("sp", "dp", None),
        P(),
        P(),
        P("sp", "dp"),
    )
    return jax.shard_map(
        functools.partial(on_device, mesh.shape["sp"]),
        mesh=mesh,
        in_specs=placed,
        out_specs=P("sp", "dp", None),
        check_vma=False,
    )
```

time: 222 us -> 176 us (0.79)
  Pallas kernels: 0 us -> 93.5 us
  blocking collectives: 62.5 us -> 0 us
  matrix products: 36.6 us -> 5.71 us
  waiting for transfers between devices: 74 us -> 54.7 us
  local copies, waits for them, and re-layouts: 19.7 us -> 5.7 us
  starting transfers between devices: 7.36 us -> 0.07 us
  other arithmetic: 7.2 us -> 2.92 us
    pallas_call x0 -> x1, Pallas kernels: none -> 93.5 us  [on_device(): pl.pallas_call(functools.partial(exchange_kernel, n, heads), out_shape=ja...]
    all_to_all x2 -> x0, waiting for transfers between devices: 73.2 us -> none  [the longest x1 40 us: on_device(): lax.all_to_all(queries.reshape(item_count, tok_rows, q_cols), 'sp', split...]
    all_to_all x2 -> x0, blocking collectives: 62.5 us -> none  [the longest x1 33.1 us: on_device(): lax.all_to_all(key_maps.reshape(item_count, tok_rows, q_cols), 'sp', spli...]
    all_gather x1, waiting for transfers between devices: 0.02 us -> 54 us  [on_device(): gathered = lax.all_gather(out_weight, 'sp', axis=0, tiled=True)]
    dot_general x33 -> x1, matrix products: 36.6 us -> 5.71 us  [on_device(): jnp.dot(gated.reshape(toks * seqs, width), lax.all_gather(gathered, 'dp',...]
    squeeze x8 -> x0, local copies, waits for them, and re-layouts: 7.44 us -> none  [on_device(): normed = lax.map(attend_one, (query_all, key_all, value_all, lambda_local))]
    all_to_all x2 -> x0, starting transfers between devices: 7.29 us -> none  [the longest x1 3.73 us: on_device(): lax.all_to_all(value_rows.reshape(item_count, tok_rows, value_cols), 'sp'...]
    dynamic_slice x8 -> x0, local copies, waits for them, and re-layouts: 4.71 us -> none  [on_device(): normed = lax.map(attend_one, (query_all, key_all, value_all, lambda_local))]
  transfers between devices with their start and end apart: 4 -> 2, of which waited for: 2 -> 1; matrix products, arithmetic and copies ran while one was open for 25% -> 4% of each run, Pallas kernels for 0% -> 53%
where the time goes in v1:
time: 176 us
  Pallas kernels  93.5 us (53%)
  waiting for transfers between devices  54.7 us (31%)
  between operations  13.5 us (8%)
  matrix products  5.71 us (3%)
  local copies, waits for them, and re-layouts  5.7 us (3%)
  other arithmetic  2.92 us (2%)
    pallas_call x1, Pallas kernels, on_device(): pl.pallas_call(functools.partial(exchange_kernel, n, heads), out_shape=ja...  93.5 us
    all_gather x1, waiting for transfers between devices, on_device(): gathered = lax.all_gather(out_weight, 'sp', axis=0, tiled=True)  54 us
    dot_general x1, matrix products, on_device(): jnp.dot(gated.reshape(toks * seqs, width), lax.all_gather(gathered, 'dp',...  5.71 us
  transfers between devices with their start and end apart: 2, of which 1 were waited for; matrix products, arithmetic and copies ran while one was open for 4% of the time, Pallas kernels for 53%

profile of v1, /device:TPU:0, one launch (start us, length us, event | category | flops | bytes accessed | tf_op | source)
XLA Modules:
  0.0 176.1 jit_solution(1369569267399774535)
XLA Ops:
  6.5 0.0 copy-start
  6.5 0.0 copy-start.1
  6.5 0.0 copy-start.4
  6.5 0.0 copy-start.3
  6.5 0.0 all-gather.3.cloned.1.call-start
  6.6 0.7 all-gather.3.cloned.1.call-update
  7.3 0.0 all-gather.5.cloned.1.call-start
  7.3 54.0 %all-gather.3.cloned.1.call-done = bf16[2048,512]{1,0:T(8,128)(2,1)} async-done(((bf16[256,512]{1,0:T(8,128)(2,1)}), bf16[2048,512]{1,0:T(8,128)(2,1)}) %all-gather.3.cloned.1.call-update) | async-done | bytes 2097168 | tf_op jit(solution)/shard_map/all_gather | solution.py:161
  61.3 0.0 all-gather.5.cloned.1.call-update
  61.3 0.0 copy-done
  61.3 0.0 copy-done.1
  61.4 0.0 copy-done.4
  61.4 0.0 copy-done.3
  61.4 0.0 copy-start.2
  61.4 1.2 copy-done.2
  62.6 93.5 %shard_map.73 = bf16[64,64,128]{2,1,0:T(8,128)(2,1)S(1)} custom-call(bf16[64,64,128]{2,1,0:T(8,128)(2,1)S(1)} %bitcast.13, bf16[64,64,128]{2,1,0:T(8,128)(2,1)S(1)} %bitcast.14, bf16[64,64,128]{2,1,0:T(8,128)(2,1)S(1)} %bitcast.15, f32[16]{0:T(128)S(1)} %copy-done.3, f32[1,128]{1,0:T(1,128)S(1)} %bitcast.16), custom_call_target="tpu_custom_call" | custom-call | flops 49999998976 | bytes 268435456 | tf_op jit(solution)/shard_map/pallas_call | solution.py:131
  156.1 0.2 convert_bitcast_fusion
  156.3 1.2 copy.8
  157.5 0.0 copy-start.5
  157.5 1.7 reshape.30
  159.3 0.0 copy-done.5
  159.3 2.7 %fusion = bf16[64,4,2048]{2,1,0:T(4,128)(2,1)S(1)} fusion(f32[64,4,2048]{2,1,0:T(4,128)} %reshape.30, bf16[64,4,2048]{2,1,0:T(4,128)(2,1)S(1)} %copy-done.5), kind=kLoop, calls=%fused_computation.3 | loop fusion | flops 3145728 | bytes 4194304 | tf_op jit(solution)/shard_map/convert_element_type | solution.py:158
  162.0 0.3 reshape.28
  162.3 0.0 all-gather.5.cloned.1.call-done
  162.3 5.7 %convolution_convert_fusion = bf16[256,2048]{1,0:T(8,128)(2,1)S(1)} fusion(bf16[256,2048]{1,0:T(8,128)(2,1)S(1)} %reshape.28, bf16[2048,2048]{1,0:T(8,128)(2,1)} %all-gather.5.cloned.1.call-done), kind=kOutput, calls=%fused_computation | convolution fusion | flops 2148007936 | bytes 10485760 | tf_op jit(solution)/shard_map/dot_general | solution.py:162
  168.0 1.2 reshape.29
Async XLA Ops:
  6.5 54.8 %copy-start = (bf16[4,16,64,128]{3,2,1,0:T(8,128)(2,1)S(1)}, bf16[4,16,64,128]{3,2,1,0:T(8,128)(2,1)}, u32[]{:S(2)}) copy-start(bf16[4,16,64,128]{3,2,1,0:T(8,128)(2,1)} %param.7) | copy-start | bytes 3145732
  6.5 54.8 %copy-start.1 = (bf16[4,16,64,128]{3,2,1,0:T(8,128)(2,1)S(1)}, bf16[4,16,64,128]{3,2,1,0:T(8,128)(2,1)}, u32[]{:S(2)}) copy-start(bf16[4,16,64,128]{3,2,1,0:T(8,128)(2,1)} %param.8) | copy-start | bytes 3145732
  6.5 54.8 %copy-start.4 = (f32[128]{0:T(128)S(1)}, f32[128]{0:T(128)}, u32[]{:S(2)}) copy-start(f32[128]{0:T(128)} %param.12) | copy-start | bytes 1540
  6.5 54.8 %copy-start.3 = (f32[16]{0:T(128)S(1)}, f32[16]{0:T(128)}, u32[]{:S(2)}) copy-start(f32[16]{0:T(128)} %lam_ref.1) | copy-start | bytes 196
  6.5 54.8 %all-gather.3.cloned.1.call-start = ((), (), s32[]{:S(2)}) async-start(), calls=%async_computation | async-start | bytes 2359296 | tf_op jit(solution)/shard_map/all_gather | solution.py:161
  7.3 155.0 %all-gather.5.cloned.1.call-start = ((), (), s32[]{:S(2)}) async-start(), calls=%async_computation.1 | async-start | bytes 10485760 | tf_op jit(solution)/shard_map/all_gather | solution.py:164
  61.4 1.2 copy-start.2
  157.5 1.8 %copy-start.5 = (bf16[64,4,2048]{2,1,0:T(4,128)(2,1)S(1)}, bf16[64,4,2048]{2,1,0:T(4,128)(2,1)}, u32[]{:S(2)}) copy-start(bf16[64,4,2048]{2,1,0:T(4,128)(2,1)} %param.10) | copy-start | bytes 3145732
Sparse Core Ops, SparseCore 0:
  9.5 51.7 all-gather.2
  62.9 56.7 all-gather.4

commit v2 on v1

--- a/solution.py
+++ b/solution.py
@@ -158,10 +158,11 @@
     gated = (jax.nn.sigmoid(gate_logits.astype(jnp.float32)) * by_token.astype(jnp.float32)).astype(
         jnp.bfloat16
     )
-    gathered = lax.all_gather(out_weight, "sp", axis=0, tiled=True)
-    result = jnp.dot(
+    gathered = lax.all_gather(out_weight, ("dp", "sp"), axis=0, tiled=True)
+    result = jnp.einsum(
+        "tk,ckn->tcn",
         gated.reshape(toks * seqs, width),
-        lax.all_gather(gathered, "dp", axis=1, tiled=True),
+        gathered.reshape(-1, width, out_weight.shape[1]),
         preferred_element_type=jnp.float32,
     )
     return result.astype(jnp.bfloat16).reshape(toks, seqs, width)

time: 176 us -> 170 us (0.966)
  waiting for transfers between devices: 54.7 us -> 0.73 us
  Pallas kernels: 93.5 us -> 136 us
  local copies, waits for them, and re-layouts: 5.7 us -> 10.5 us
    all_gather x2 -> x1, waiting for transfers between devices: 54 us -> 0.02 us  [on_device(): gathered = lax.all_gather(out_weight, ('dp', 'sp'), axis=0, tiled=True)]
    pallas_call x1, Pallas kernels: 93.5 us -> 136 us  [on_device(): pl.pallas_call(functools.partial(exchange_kernel, n, heads), out_shape=ja...]
    unnamed x12, local copies, waits for them, and re-layouts: 1.24 us -> 4.98 us
  transfers between devices with their start and end apart: 2 -> 1, of which waited for: 1 -> 0; matrix products, arithmetic and copies ran while one was open for 4% -> 4% of each run, Pallas kernels for 53% -> 80%
where the time goes in v2:
time: 170 us
  Pallas kernels  136 us (80%)
  between operations  13.5 us (8%)
  local copies, waits for them, and re-layouts  10.5 us (6%)
  matrix products  5.7 us (3%)
  other arithmetic  2.93 us (2%)
    pallas_call x1, Pallas kernels, on_device(): pl.pallas_call(functools.partial(exchange_kernel, n, heads), out_shape=ja...  136 us
    dot_general x1, matrix products, on_device(): jnp.einsum('tk,ckn->tcn', gated.reshape(toks * seqs, width), gathered.res...  5.7 us
    unnamed x12, local copies, waits for them, and re-layouts  4.98 us
  transfers between devices with their start and end apart: 1, of which 0 were waited for; matrix products, arithmetic and copies ran while one was open for 4% of the time, Pallas kernels for 80%

profile of v2, /device:TPU:0, one launch (start us, length us, event | category | flops | bytes accessed | tf_op | source)
XLA Modules:
  0.0 169.6 jit_solution(16107531002783766022)
XLA Ops:
  6.5 0.0 all-gather.2.cloned.1.call-start
  6.5 0.7 all-gather.2.cloned.1.call-update
  7.3 0.0 copy-start
  7.3 1.2 copy-done
  8.5 0.0 copy-start.1
  8.5 1.2 copy-done.1
  9.7 0.0 copy-start.2
  9.7 1.2 copy-done.2
  10.9 0.0 copy-start.3
  10.9 0.7 copy-done.3
  11.6 0.0 copy-start.4
  11.6 0.7 copy-done.4
  12.2 136.3 %shard_map.73 = bf16[64,64,128]{2,1,0:T(8,128)(2,1)S(1)} custom-call(bf16[64,64,128]{2,1,0:T(8,128)(2,1)S(1)} %bitcast.14, bf16[64,64,128]{2,1,0:T(8,128)(2,1)S(1)} %bitcast.15, bf16[64,64,128]{2,1,0:T(8,128)(2,1)S(1)} %bitcast.16, f32[16]{0:T(128)S(1)} %copy-done.3, f32[1,128]{1,0:T(1,128)S(1)} %bitcast.17), custom_call_target="tpu_custom_call" | custom-call | flops 49999998976 | bytes 268435456 | tf_op jit(solution)/shard_map/pallas_call | solution.py:131
  148.5 0.2 convert_bitcast_fusion
  148.8 1.2 copy.9
  150.0 0.0 copy-start.5
  150.0 1.7 %reshape.34 = f32[64,4,2048]{2,1,0:T(4,128)} reshape(f32[64,4,16,128]{3,2,1,0:T(8,128)S(1)} %copy.9) | data formatting | bytes 4194304 | tf_op jit(solution)/shard_map/convert_element_type | solution.py:158
  151.7 0.0 copy-done.5
  151.7 2.7 %fusion = bf16[64,4,2048]{2,1,0:T(4,128)(2,1)S(1)} fusion(f32[64,4,2048]{2,1,0:T(4,128)} %reshape.34, bf16[64,4,2048]{2,1,0:T(4,128)(2,1)S(1)} %copy-done.5), kind=kLoop, calls=%fused_computation.2 | loop fusion | flops 3145728 | bytes 4194304 | tf_op jit(solution)/shard_map/convert_element_type | solution.py:158
  154.4 0.3 reshape.36
  154.7 0.0 all-gather.2.cloned.1.call-done
  154.8 5.7 %convolution_convert_fusion = bf16[256,4,512]{2,0,1:T(8,128)(2,1)S(1)} fusion(bf16[256,2048,1]{1,0,2:T(8,128)(2,1)S(1)} %reshape.36, bf16[4,2048,512]{2,1,0:T(8,128)(2,1)} %bitcast.18), kind=kOutput, calls=%fused_computation.3 | convolution fusion | flops 2148007936 | bytes 10485760 | tf_op jit(solution)/shard_map/tk,ckn->tcn/dot_general | solution.py:162
  160.5 0.8 copy.10
  161.3 1.5 reshape.33
Async XLA Ops:
  6.5 148.2 %all-gather.2.cloned.1.call-start = ((), (), s32[]{:S(2)}) async-start(), calls=%async_computation | async-start | bytes 8650752 | tf_op jit(solution)/shard_map/all_gather | solution.py:161
  7.3 1.2 copy-start
  8.5 1.2 copy-start.1
  9.7 1.2 copy-start.2
  10.9 0.7 copy-start.3
  11.6 0.7 copy-start.4
  150.0 1.8 %copy-start.5 = (bf16[64,4,2048]{2,1,0:T(4,128)(2,1)S(1)}, bf16[64,4,2048]{2,1,0:T(4,128)(2,1)}, u32[]{:S(2)}) copy-start(bf16[64,4,2048]{2,1,0:T(4,128)(2,1)} %param.10) | copy-start | bytes 3145732
Sparse Core Ops, SparseCore 0:
  10.3 118.7 all-gather.1
